TPU v7x, 512 devices: a whole 4x8x8 slice. The times are simulated.
512 devices in a mesh: sp: 128 (over z, y, core), tp: 4 (over x).
Axes of the slice: x: 4, y: 8, z: 8, core: 2. Of those that a mesh axis runs over, the one named last changes fastest.
Arguments:
- tokens: bfloat16 [65536, 2048], P('sp'), may hold values from -24 to 24
- w_query: bfloat16 [2048, 1536], P('sp', 'tp'), as said below
- w_key: bfloat16 [2048, 1536], P('sp', 'tp'), as said below
- w_value: bfloat16 [2048, 1536], P('sp', 'tp'), may hold values from -0.125 to 0.125
- w_out: bfloat16 [512, 2048], P('tp', 'sp'), may hold values from -1.5 to 1.5
Outputs:
- mixed: bfloat16 [65536, 2048], P(('sp', 'tp'))
Inputs may be any that keep to these rules, and one draw needn't show every extreme that they name: `w_query`: every entry lies within 4 / sqrt(2048) of zero. `w_key`: every entry lies within 4 / sqrt(2048) of zero.
All inputs are finite; a program needn't handle non-finite values.
Results may differ from a plain program's by a relative error of at most 0.025.
Values may be sent and summed in bfloat16 or wider, within the bound.
No kernel may reach another device: no remote copies, remote signals or barrier semaphores. Data moves between devices by JAX's collectives and lax.ppermute only.
A program may use at most 64 MiB of HBM per device.

v0:
```python
import math

import jax
import jax.numpy as jnp
from jax import lax
from jax.sharding import PartitionSpec as P

GROUPS = 3
DH = 128
WIN1 = 128
WIN2 = 512
WIN3 = 2048
SECOND_DILATION = 4
THIRD_DILATION = 16


ROPE_BASE = 500000.0


def from_behind(block, axis, distance):
    devices = range(lax.axis_size(axis))
    route = [(i - distance, i) for i in devices if i - distance in devices]
    return lax.ppermute(block, axis, route)


def sent_together(arrays, axis, dim, along):
    widths = [a.shape[along] for a in arrays]
    both = jnp.concatenate(arrays, axis=along)
    filled = lax.all_gather(both, axis, axis=dim, tiled=True)
    return tuple(jnp.split(filled, [sum(widths[:k]) for k in range(1, len(widths))], axis=along))


def joined_along(pieces, dim):
    lengths = list(pieces.shape[1:])
    lengths[dim] *= pieces.shape[0]
    return jnp.moveaxis(pieces, 0, dim).reshape(lengths)


def from_everyone(value, axis):
    copies = jnp.broadcast_to(value, (lax.axis_size(axis), *value.shape))
    return lax.all_to_all(copies, axis, split_axis=0, concat_axis=0, tiled=True)


def gather_directly(value, axis, dim):
    return joined_along(from_everyone(value, axis), dim)


def rotate(projected, offset):
    tok_rows = projected.shape[0]
    head_size = projected.shape[-1]
    half_size = head_size // 2
    positions = (offset + jnp.arange(tok_rows, dtype=jnp.int32)).astype(jnp.float32)
    frequency = 1.0 / ROPE_BASE ** (jnp.arange(0, head_size, 2, dtype=jnp.float32) / head_size)
    angles = (positions[:, None] * frequency[None, :]).reshape(tok_rows, 1, 1, half_size)
    cosine = jnp.cos(angles)
    sine_part = jnp.sin(angles)
    first_half = projected[..., :half_size]
    second_half = projected[..., half_size:]
    return jnp.concatenate(
        [
            first_half * cosine - second_half * sine_part,
            second_half * cosine + first_half * sine_part,
        ],
        axis=-1,
    )


def window_attend(query_part, buffer, steps, stride, offset):
    tok_rows, heads_here, head_size = query_part.shape
    sub_rows = tok_rows // stride
    key_rows = buffer.shape[1] // stride
    query_sub = query_part.reshape(sub_rows, stride, heads_here, head_size).transpose(1, 2, 0, 3)
    pair_sub = buffer.reshape(2, key_rows, stride, heads_here, head_size).transpose(0, 2, 3, 1, 4)
    block_rows = math.gcd(sub_rows, steps) if sub_rows > steps else sub_rows
    block_list = sub_rows // block_rows
    query_blocks = query_sub.reshape(stride, heads_here, block_list, block_rows, head_size)
    key_blocks = jnp.stack(
        [
            pair_sub[:, :, :, index * block_rows : index * block_rows + block_rows + steps]
            for index in range(block_list)
        ],
        axis=3,
    )
    scores = jnp.einsum(
        "zhnqe,zhnke->zhnqk", query_blocks, key_blocks[0], preferred_element_type=jnp.float32
    ) * head_size ** (-0.5)
    query_index = (jnp.arange(block_list, dtype=jnp.int32) * block_rows)[
        :, None, None
    ] + jnp.arange(block_rows, dtype=jnp.int32)[None, :, None]
    key_index = (jnp.arange(block_list, dtype=jnp.int32) * block_rows)[:, None, None] + jnp.arange(
        block_rows + steps, dtype=jnp.int32
    )[None, None, :]
    spacing = query_index + steps - key_index
    residue = jnp.arange(stride, dtype=jnp.int32)[:, None, None, None]
    key_position = offset + (key_index[None] - steps) * stride + residue
    allowed = (spacing[None] >= 0) & (spacing[None] <= steps) & (key_position >= 0)
    scores = jnp.where(allowed[:, None], scores, -jnp.inf)
    row_max = jnp.max(scores, axis=-1)
    exponent = jnp.exp(scores - row_max[..., None])
    totals = jnp.sum(exponent, axis=-1)
    probs = (exponent / totals[..., None]).astype(jnp.bfloat16)
    mixed = jnp.einsum(
        "zhnqk,zhnke->zhnqe", probs, key_blocks[1], preferred_element_type=jnp.float32
    )
    mixed = mixed.reshape(stride, heads_here, sub_rows, head_size).transpose(2, 0, 1, 3)
    log_total = (row_max + jnp.log(totals)).reshape(stride, heads_here, sub_rows).transpose(2, 0, 1)
    return (mixed.reshape(tok_rows, heads_here, head_size), log_total.reshape(tok_rows, heads_here))


def reach_back(key_value, distance_max):
    earlier = [from_behind(key_value, "sp", distance) for distance in range(distance_max, 0, -1)]
    return jnp.concatenate(earlier + [key_value], axis=1)


def on_device(tokens, w_query, w_key, w_value, w_out):
    tok_rows = tokens.shape[0]
    heads_here = w_out.shape[0] // DH
    offset = lax.axis_index("sp") * tok_rows
    weight_parts = sent_together((w_query, w_key, w_value), "sp", 0, 1)
    query_raw, key_raw, value_raw = tuple(
        (
            jnp.dot(tokens, weight_rows, preferred_element_type=jnp.float32)
            for weight_rows in weight_parts
        )
    )
    head_shape = (tok_rows, heads_here, GROUPS, DH)
    queries = rotate(query_raw.reshape(head_shape), offset).astype(jnp.bfloat16)
    keys_all = rotate(key_raw.reshape(head_shape), offset).astype(jnp.bfloat16)
    values_all = value_raw.astype(jnp.bfloat16).reshape(head_shape)
    windows = (WIN1, WIN2, WIN3)
    step_sizes = (1, SECOND_DILATION, THIRD_DILATION)
    outputs = []
    log_totals = []
    for group_index in range(GROUPS):
        key_value = jnp.stack([keys_all[:, :, group_index], values_all[:, :, group_index]])
        key_value = key_value.reshape(2, tok_rows, heads_here * DH)
        window = windows[group_index]
        if group_index == 0:
            near_rows = from_behind(key_value[:, tok_rows - window :], "sp", 1)
            buffer = jnp.concatenate([near_rows, key_value], axis=1)
        else:
            distance_max = (window + tok_rows - 1) // tok_rows
            buffer = reach_back(key_value, distance_max)
        group_out, log_total = window_attend(
            queries[:, :, group_index],
            buffer,
            window // step_sizes[group_index],
            step_sizes[group_index],
            offset,
        )
        outputs.append(group_out)
        log_totals.append(log_total)
    group_weights = jax.nn.softmax(jnp.stack(log_totals), axis=0)
    merged = jnp.sum(group_weights[..., None] * jnp.stack(outputs), axis=0).astype(jnp.bfloat16)
    merged = merged.reshape(tok_rows, heads_here * DH)
    by_position = lax.all_to_all(merged, "tp", split_axis=0, concat_axis=1, tiled=True)
    all_rows = gather_directly(w_out, "tp", 0)
    summed = jnp.dot(
        by_position,
        lax.all_gather(all_rows, "sp", axis=1, tiled=True),
        preferred_element_type=jnp.float32,
    )
    return summed.astype(jnp.bfloat16)


def solution(mesh):
    placed = (P("sp", None), P("sp", "tp"), P("sp", "tp"), P("sp", "tp"), P("tp", "sp"))
    return jax.shard_map(
        on_device, mesh=mesh, in_specs=placed, out_specs=P(("sp", "tp"), None), check_vma=False
    )
```

profile of v0, /device:TPU:1, one launch (start us, length us, event | category | flops | bytes accessed | tf_op | source)
XLA Modules:
  0.0 195.9 jit_solution(5047055239080944040)
XLA Ops:
  6.5 1.5 pad_maximum_fusion.4
  8.1 1.3 broadcast_in_dim.11
  9.4 4.8 %all-to-all-start.1 = ((bf16[4,128,16]{1,2,0:T(8,128)(2,1)}), bf16[4,128,16]{1,2,0:T(8,128)(2,1)S(1)}, u32[]{:S(2)}, u32[]{:S(2)}) async-start(bf16[4,128,16]{1,2,0:T(8,128)(2,1)} %broadcast_in_dim.11), calls=%async_computation.1 | async-start | bytes 32768 | tf_op jit(solution)/shard_map/all_to_all | solution.py:41
  16.4 1.8 multiply_cosine_fusion
  19.5 81.9 %all-gather.3.cloned.1.call-done = bf16[2048,1152]{1,0:T(8,128)(2,1)} async-done(((bf16[16,1152]{1,0:T(8,128)(2,1)}), bf16[2048,1152]{1,0:T(8,128)(2,1)}) %all-gather.3.cloned.1.call-update) | async-done | bytes 4718608 | tf_op jit(solution)/shard_map/all_gather | solution.py:29
  101.4 2.4 %fusion.6 = bf16[384,512]{1,0:T(8,128)(2,1)S(1)} fusion(bf16[512,2048]{1,0:T(8,128)(2,1)S(1)} %copy-done, bf16[2048,1152]{1,0:T(8,128)(2,1)} %all-gather.3.cloned.1.call-done), kind=kOutput, calls=%fused_computation.8 | convolution fusion | flops 805502976 | bytes 4063232 | tf_op jit(solution)/shard_map/dot_general | solution.py:122
  104.6 2.4 %fusion.4 = f32[384,512]{1,0:T(8,128)S(1)} fusion(bf16[512,2048]{1,0:T(8,128)(2,1)S(1)} %copy-done, bf16[2048,1152]{1,0:T(8,128)(2,1)} %all-gather.3.cloned.1.call-done), kind=kOutput, calls=%fused_computation.5 | convolution fusion | flops 805306368 | bytes 4456448 | tf_op jit(solution)/shard_map/dot_general | solution.py:122
  107.9 1.3 copy.112
  109.1 1.2 copy.111
  110.3 2.4 %fusion.2 = f32[384,512]{1,0:T(8,128)S(1)} fusion(bf16[512,2048]{1,0:T(8,128)(2,1)S(1)} %copy-done, bf16[2048,1152]{1,0:T(8,128)(2,1)} %all-gather.3.cloned.1.call-done), kind=kOutput, calls=%fused_computation.3 | convolution fusion | flops 805306368 | bytes 4456448 | tf_op jit(solution)/shard_map/dot_general | solution.py:122
  113.5 2.2 %copy.113 = f32[512,1,3,64]{3,0,2,1:T(8,128)} copy(f32[512,1,3,64]{0,3,2,1:T(8,128)} %get-tuple-element.20) | data formatting | bytes 786432
  115.7 1.2 copy.114
  116.9 2.2 %subtract_convert_fusion.1 = (bf16[512,1,3,64]{3,0,2,1:T(8,128)(2,1)S(1)}, bf16[512,1,3,64]{3,0,2,1:T(8,128)(2,1)S(1)}, bf16[512,1,3,64]{3,0,2,1:T(8,128)(2,1)S(1)}, bf16[512,1,3,64]{3,0,2,1:T(8,128)(2,1)S(1)}) fusion(f32[512,1,3,64]{3,0,2,1:T(8,128)S(1)} %copy.112, f32[512,1,3,64]{3,0,2,1:T(8,128)} %copy.111, f32[512,64]{1,0:T(8,128)} %get-tuple-element.31, ...), kind=kLoop, calls=%fused_computation.22 | loop fusion | flops 1572864 | bytes 2621440 | tf_op jit(solution)/shard_map/convert.2
  119.1 1.2 fusion.27
  121.0 4.6 %collective-permute-start.2 = (bf16[2,512,128]{2,1,0:T(8,128)(2,1)}, bf16[2,512,128]{2,1,0:T(8,128)(2,1)}, u32[]{:S(2)}, u32[]{:S(2)}) collective-permute-start(bf16[2,512,128]{2,1,0:T(8,128)(2,1)} %maximum_bitcast_fusion.3), channel_id=1, source_target_pairs={{0,16},{4,20},{8,24},{12,28},{16,32},{20,36},{24,40},{28,44},{32,4... | collective-permute-start | bytes 786440 | tf_op jit(solution)/shard_map/ppermute | solution.py:23
  125.6 4.5 %collective-permute-start.3 = (bf16[2,512,128]{2,1,0:T(8,128)(2,1)}, bf16[2,512,128]{2,1,0:T(8,128)(2,1)}, u32[]{:S(2)}, u32[]{:S(2)}) collective-permute-start(bf16[2,512,128]{2,1,0:T(8,128)(2,1)} %maximum_bitcast_fusion.3), channel_id=1, source_target_pairs={{0,12},{4,16},{8,20},{12,24},{16,28},{20,32},{24,36},{28,40},{32,4... | collective-permute-start | bytes 786440 | tf_op jit(solution)/shard_map/ppermute | solution.py:23
  130.1 2.1 %collective-permute-start.4 = (bf16[2,512,128]{2,1,0:T(8,128)(2,1)}, bf16[2,512,128]{2,1,0:T(8,128)(2,1)}, u32[]{:S(2)}, u32[]{:S(2)}) collective-permute-start(bf16[2,512,128]{2,1,0:T(8,128)(2,1)} %maximum_bitcast_fusion.3), channel_id=1, source_target_pairs={{0,8},{4,12},{8,16},{12,20},{16,24},{20,28},{24,32},{28,36},{32,40... | collective-permute-start | bytes 786440 | tf_op jit(solution)/shard_map/ppermute | solution.py:23
  132.2 1.9 collective-permute-start.5
  134.4 2.0 collective-permute-start
  137.1 17.7 %collective-permute-done = bf16[2,128,128]{2,1,0:T(8,128)(2,1)S(1)} collective-permute-done((bf16[2,128,128]{2,1,0:T(8,128)(2,1)S(1)}, bf16[2,128,128]{2,1,0:T(8,128)(2,1)S(1)}, u32[]{:S(2)}, u32[]{:S(2)}) %collective-permute-start) | collective-permute-done | bytes 65568 | tf_op jit(solution)/shard_map/ppermute | solution.py:23
  154.8 4.4 %collective-permute-start.1 = (bf16[2,512,128]{2,1,0:T(8,128)(2,1)}, bf16[2,512,128]{2,1,0:T(8,128)(2,1)}, u32[]{:S(2)}, u32[]{:S(2)}) collective-permute-start(bf16[2,512,128]{2,1,0:T(8,128)(2,1)} %maximum_bitcast_fusion.2), channel_id=1, source_target_pairs={{0,4},{4,8},{8,12},{12,16},{16,20},{20,24},{24,28},{28,32},{32,36}... | collective-permute-start | bytes 786440 | tf_op jit(solution)/shard_map/ppermute | solution.py:23
  160.0 1.1 fusion.18
  161.1 1.0 constant_dynamic-update-slice_fusion.4
  162.1 1.0 constant_dynamic-update-slice_fusion.3
  163.1 1.0 constant_dynamic-update-slice_fusion.2
  164.1 1.0 constant_dynamic-update-slice_fusion.1
  168.0 1.1 pad_maximum_fusion.1
  169.1 1.4 fusion.50
  171.9 1.5 convolution_bitcast_fusion
  174.8 8.7 %all_to_all.21 = bf16[4,128,128]{2,1,0:T(8,128)(2,1)S(1)} all-to-all(bf16[4,128,128]{2,1,0:T(8,128)(2,1)S(1)} %bitcast.152), channel_id=1, replica_groups=mesh['sp'=128,'tp'=4] {'tp'}, dimensions={0} | all-to-all | bytes 262144 | tf_op jit(solution)/shard_map/all_to_all | solution.py:156
  183.6 2.3 %all-gather.5.cloned.1.call-done = bf16[512,2048]{0,1:T(8,128)(2,1)} async-done(((bf16[512,16]{0,1:T(8,128)(2,1)}), bf16[512,2048]{0,1:T(8,128)(2,1)}) %all-gather.5.cloned.1.call-update) | async-done | bytes 2097168 | tf_op jit(solution)/shard_map/all_gather | solution.py:160
  185.9 3.2 %convolution_convert_fusion = bf16[128,2048]{1,0:T(8,128)(2,1)} fusion(bf16[128,512]{0,1:T(8,128)(2,1)S(1)} %bitcast.158, bf16[512,2048]{0,1:T(8,128)(2,1)} %all-gather.5.cloned.1.call-done), kind=kOutput, calls=%fused_computation | convolution fusion | flops 268697600 | bytes 2752512 | tf_op jit(solution)/shard_map/dot_general | solution.py:158
  (92 shorter events, 14.1 us)
Async XLA Ops:
  6.5 94.8 %copy-start = (bf16[512,2048]{1,0:T(8,128)(2,1)S(1)}, bf16[512,2048]{1,0:T(8,128)(2,1)}, u32[]{:S(2)}) copy-start(bf16[512,2048]{1,0:T(8,128)(2,1)} %param.5) | copy-start | bytes 6291460
  6.5 94.8 %all-gather.3.cloned.1.call-start = ((), (), s32[]{:S(2)}) async-start(), calls=%async_computation.2 | async-start | bytes 4755456 | tf_op jit(solution)/shard_map/all_gather | solution.py:29
  9.4 9.5 %all-to-all-start.1 = ((bf16[4,128,16]{1,2,0:T(8,128)(2,1)}), bf16[4,128,16]{1,2,0:T(8,128)(2,1)S(1)}, u32[]{:S(2)}, u32[]{:S(2)}) async-start(bf16[4,128,16]{1,2,0:T(8,128)(2,1)} %broadcast_in_dim.11), calls=%async_computation.1 | async-start | bytes 32768 | tf_op jit(solution)/shard_map/all_to_all | solution.py:41
  14.2 171.7 %all-gather.5.cloned.1.call-start = ((), (), s32[]{:S(2)}) async-start(), calls=%async_computation.3 | async-start | bytes 2113536 | tf_op jit(solution)/shard_map/all_gather | solution.py:160
  119.1 15.0 %copy-start.6 = (bf16[512,1,1,128]{0,3,2,1:T(8,128)(2,1)S(1)}, bf16[512,1,1,128]{0,3,2,1:T(8,128)(2,1)}, u32[]{:S(2)}) copy-start(bf16[512,1,1,128]{0,3,2,1:T(8,128)(2,1)} %get-tuple-element.24) | copy-start | bytes 393220
  121.0 40.1 %collective-permute-start.2 = (bf16[2,512,128]{2,1,0:T(8,128)(2,1)}, bf16[2,512,128]{2,1,0:T(8,128)(2,1)}, u32[]{:S(2)}, u32[]{:S(2)}) collective-permute-start(bf16[2,512,128]{2,1,0:T(8,128)(2,1)} %maximum_bitcast_fusion.3), channel_id=1, source_target_pairs={{0,16},{4,20},{8,24},{12,28},{16,32},{20,36},{24,40},{28,44},{32,4... | collective-permute-start | bytes 786440 | tf_op jit(solution)/shard_map/ppermute | solution.py:23
  125.6 36.5 %collective-permute-start.3 = (bf16[2,512,128]{2,1,0:T(8,128)(2,1)}, bf16[2,512,128]{2,1,0:T(8,128)(2,1)}, u32[]{:S(2)}, u32[]{:S(2)}) collective-permute-start(bf16[2,512,128]{2,1,0:T(8,128)(2,1)} %maximum_bitcast_fusion.3), channel_id=1, source_target_pairs={{0,12},{4,16},{8,20},{12,24},{16,28},{20,32},{24,36},{28,40},{32,4... | collective-permute-start | bytes 786440 | tf_op jit(solution)/shard_map/ppermute | solution.py:23
  130.1 33.0 %collective-permute-start.4 = (bf16[2,512,128]{2,1,0:T(8,128)(2,1)}, bf16[2,512,128]{2,1,0:T(8,128)(2,1)}, u32[]{:S(2)}, u32[]{:S(2)}) collective-permute-start(bf16[2,512,128]{2,1,0:T(8,128)(2,1)} %maximum_bitcast_fusion.3), channel_id=1, source_target_pairs={{0,8},{4,12},{8,16},{12,20},{16,24},{20,28},{24,32},{28,36},{32,40... | collective-permute-start | bytes 786440 | tf_op jit(solution)/shard_map/ppermute | solution.py:23
  132.2 31.9 %collective-permute-start.5 = (bf16[2,512,128]{2,1,0:T(8,128)(2,1)}, bf16[2,512,128]{2,1,0:T(8,128)(2,1)}, u32[]{:S(2)}, u32[]{:S(2)}) collective-permute-start(bf16[2,512,128]{2,1,0:T(8,128)(2,1)} %maximum_bitcast_fusion.3), channel_id=1, source_target_pairs={{0,4},{4,8},{8,12},{12,16},{16,20},{20,24},{24,28},{28,32},{32,36}... | collective-permute-start | bytes 786440 | tf_op jit(solution)/shard_map/ppermute | solution.py:23
  134.4 20.4 %collective-permute-start = (bf16[2,128,128]{2,1,0:T(8,128)(2,1)S(1)}, bf16[2,128,128]{2,1,0:T(8,128)(2,1)S(1)}, u32[]{:S(2)}, u32[]{:S(2)}) collective-permute-start(bf16[2,128,128]{2,1,0:T(8,128)(2,1)S(1)} %slice.109), channel_id=1, source_target_pairs={{0,4},{4,8},{8,12},{12,16},{16,20},{20,24},{24,28},{28,32},{32,36}... | collective-permute-start | bytes 196616 | tf_op jit(solution)/shard_map/ppermute | solution.py:23
  136.4 23.0 %copy-start.9 = (bf16[512,1,1,128]{3,0,2,1:T(8,128)(2,1)S(1)}, bf16[512,1,1,128]{3,0,2,1:T(8,128)(2,1)}, u32[]{:S(2)}) copy-start(bf16[512,1,1,128]{3,0,2,1:T(8,128)(2,1)} %get-tuple-element.40) | copy-start | bytes 393220
  136.4 23.0 %copy-start.11 = (s32[4,128]{1,0:T(4,128)S(1)}, s32[4,128]{1,0:T(4,128)}, u32[]{:S(2)}) copy-start(s32[4,128]{1,0:T(4,128)} %add_add_fusion) | copy-start | bytes 6148
  136.4 23.0 %copy-start.13 = (pred[4,256]{1,0:T(4,128)(4,1)S(1)}, pred[4,256]{1,0:T(4,128)(4,1)}, u32[]{:S(2)}) copy-start(pred[4,256]{1,0:T(4,128)(4,1)} %add_compare_fusion.2) | copy-start | bytes 3076
  154.8 13.1 %collective-permute-start.1 = (bf16[2,512,128]{2,1,0:T(8,128)(2,1)}, bf16[2,512,128]{2,1,0:T(8,128)(2,1)}, u32[]{:S(2)}, u32[]{:S(2)}) collective-permute-start(bf16[2,512,128]{2,1,0:T(8,128)(2,1)} %maximum_bitcast_fusion.2), channel_id=1, source_target_pairs={{0,4},{4,8},{8,12},{12,16},{16,20},{20,24},{24,28},{28,32},{32,36}... | collective-permute-start | bytes 786440 | tf_op jit(solution)/shard_map/ppermute | solution.py:23
  165.1 0.9 copy-start.8
  166.6 0.8 copy-start.1
  166.6 2.5 %copy-start.10 = (pred[128,256]{1,0:T(8,128)(4,1)S(1)}, pred[128,256]{1,0:T(8,128)(4,1)}, u32[]{:S(2)}) copy-start(pred[128,256]{1,0:T(8,128)(4,1)} %fusion.37) | copy-start | bytes 98308
  166.6 2.5 %copy-start.12 = (pred[4,256]{1,0:T(4,128)(4,1)S(1)}, pred[4,256]{1,0:T(4,128)(4,1)}, u32[]{:S(2)}) copy-start(pred[4,256]{1,0:T(4,128)(4,1)} %add_compare_fusion.1) | copy-start | bytes 3076
  169.1 1.7 copy-start.2
  170.5 0.8 copy-start.4
  171.9 1.7 copy-start.3
  171.9 1.7 copy-start.5
  173.6 1.0 copy-start.7
Sparse Core Ops, SparseCore 0:
  10.5 90.8 all-gather.2
  104.5 81.3 all-gather.4
where the time goes:
time: 197 us; the launch traced here: 196 us
  waiting for transfers between devices  102 us (52%)
  starting transfers between devices  24.3 us (12%)
  local copies, waits for them, and re-layouts  18.2 us (9%)
  matrix products  15.7 us (8%)
  between operations  13.9 us (7%)
  other arithmetic  13.3 us (7%)
  blocking collectives  8.72 us (4%)
    all_gather x1, waiting for transfers between devices, sent_together(): filled = lax.all_gather(both, axis, axis=dim, tiled=True)  81.9 us
    ppermute x6, starting transfers between devices, from_behind(): return lax.ppermute(block, axis, route)  19.5 us
    ppermute x6, waiting for transfers between devices, from_behind(): return lax.ppermute(block, axis, route)  17.7 us
    unnamed x39, local copies, waits for them, and re-layouts  12.3 us
    all_to_all x1, blocking collectives, on_device(): lax.all_to_all(merged, 'tp', split_axis=0, concat_axis=1, tiled=True)  8.72 us
    dot_general x3, matrix products, on_device(): jnp.dot(tokens, weight_rows, preferred_element_type=jnp.float32)  7.28 us
    all_to_all x1, starting transfers between devices, from_everyone(): return lax.all_to_all(copies, axis, split_axis=0, concat_axis=0, tiled=True)  4.83 us
  transfers between devices with their start and end apart: 9, of which 3 were waited for; matrix products, arithmetic and copies ran while one was open for 21% of the time, Pallas kernels for 0%

commit v1 on v0

v1 whole, which is shorter than its diff:
```python
import functools

import jax
import jax.numpy as jnp
from jax import lax
from jax.experimental import pallas as pl
from jax.experimental.pallas import tpu as pltpu
from jax.sharding import Mesh
from jax.sharding import PartitionSpec as P

DH = 128
ROWS = 512
ROPE_BASE = 500000.0
SP = ("z", "y", "core")
F32 = jnp.float32
BF16 = jnp.bfloat16
SCALE = DH ** (-0.5)
MIB = 1024 * 1024


def spread(value, axis):
    copies = jnp.broadcast_to(value, (lax.axis_size(axis), *value.shape))
    return lax.all_to_all(copies, axis, split_axis=0, concat_axis=0, tiled=True)


def from_behind(block, distance):
    size = lax.axis_size(SP)
    return lax.ppermute(block, SP, [(i - distance, i) for i in range(distance, size)])


def from_partner(block):
    return lax.ppermute(block, "core", [(0, 1), (1, 0)])


def call(body, outs, scratch=(), flops=0, moved=0, name=None, in_specs=None):
    extra = {} if in_specs is None else {"in_specs": in_specs}
    return pl.pallas_call(
        body,
        out_shape=outs,
        scratch_shapes=list(scratch),
        compiler_params=pltpu.CompilerParams(vmem_limit_bytes=48 * MIB),
        cost_estimate=pl.CostEstimate(flops=flops, bytes_accessed=moved, transcendentals=0),
        name=name,
        **extra,
    )


def tables(offset):
    positions = (offset + jnp.arange(ROWS, dtype=jnp.int32)).astype(F32)
    frequency = 1.0 / ROPE_BASE ** (jnp.arange(0, DH, 2, dtype=F32) / DH)
    angles = positions[:, None] * frequency[None, :]
    cosine, sine = jnp.cos(angles), jnp.sin(angles)
    return jnp.concatenate([cosine, cosine], axis=1), jnp.concatenate([-sine, sine], axis=1)


def turned(raw, cos_ref, sin_ref):
    return raw * cos_ref[...] + pltpu.roll(raw, DH // 2, 1) * sin_ref[...]


def reorder_body(tok_ref, out_ref):
    row = lax.broadcasted_iota(jnp.int32, (256, 256), 0)
    col = lax.broadcasted_iota(jnp.int32, (256, 256), 1)
    target = ((row >> 4) & 1) * 128 + (row >> 5) * 16 + (row & 15)
    moves = (col == target).astype(BF16)
    for z in range(8):
        part = tok_ref[:, z * 256 : (z + 1) * 256]
        out_ref[:, z * 256 : (z + 1) * 256] = jnp.dot(part, moves, preferred_element_type=F32).astype(BF16)


def by_residue(value, stage_ref, out_ref, base, stride):
    stage_ref[...] = value
    count = ROWS // stride
    for r in range(stride):
        out_ref[base + r * count : base + (r + 1) * count, :] = stage_ref[
            pl.ds(r, count, stride=stride), :
        ].astype(BF16)


def kv3_body(tok_ref, w_ref, cos_ref, sin_ref, out_ref, stage_ref):
    acc = jnp.zeros((ROWS, 2 * DH), F32)
    for z in range(8):
        rows = jnp.concatenate([w_ref[0, z], w_ref[1, z]], axis=0)
        acc = acc + jnp.dot(tok_ref[:, z * 256 : (z + 1) * 256], rows, preferred_element_type=F32)
    by_residue(turned(acc[:, :DH], cos_ref, sin_ref), stage_ref, out_ref, 0, 16)
    by_residue(acc[:, DH:], stage_ref, out_ref, ROWS, 16)


def kv12_body(tok_ref, w_ref, cos_ref, sin_ref, own_ref, send_ref, stage_ref):
    keys = jnp.dot(tok_ref[...], w_ref[:, : 2 * DH], preferred_element_type=F32)
    near = turned(keys[:, :DH], cos_ref, sin_ref).astype(BF16)
    own_ref[:ROWS] = near
    send_ref[:128] = near[ROWS - 128 :]
    by_residue(turned(keys[:, DH:], cos_ref, sin_ref), stage_ref, send_ref, 256, 4)
    values = jnp.dot(tok_ref[...], w_ref[:, 2 * DH :], preferred_element_type=F32)
    near = values[:, :DH].astype(BF16)
    own_ref[ROWS:] = near
    send_ref[128:256] = near[ROWS - 128 :]
    by_residue(values[:, DH:], stage_ref, send_ref, 256 + ROWS, 4)


def attend(query, key, value, allowed):
    scores = lax.dot_general(query, key, (((1,), (1,)), ((), ())), preferred_element_type=F32) * SCALE
    scores = jnp.where(allowed, scores, -jnp.inf)
    top = jnp.max(scores, axis=-1, keepdims=True)
    weight = jnp.exp(scores - top)
    total = jnp.sum(weight, axis=-1, keepdims=True)
    probs = (weight * (1.0 / total)).astype(BF16)
    return jnp.dot(probs, value, preferred_element_type=F32), top + jnp.log(total)


def q_body(spi_ref, tok_ref, w_ref, cos_ref, sin_ref, x4, x3, x2, x1, x0, q_ref, out_ref, log_ref, stage_ref, q3_ref):
    spi = spi_ref[0, 0]
    first = jnp.dot(tok_ref[...], w_ref[:, : 2 * DH], preferred_element_type=F32)
    q_ref[:ROWS] = turned(first[:, :DH], cos_ref, sin_ref).astype(BF16)
    by_residue(turned(first[:, DH:], cos_ref, sin_ref), stage_ref, q_ref, ROWS, 4)
    third = jnp.dot(tok_ref[...], w_ref[:, 2 * DH : 3 * DH], preferred_element_type=F32)
    by_residue(turned(third, cos_ref, sin_ref), stage_ref, q3_ref, 0, 16)
    row = lax.broadcasted_iota(jnp.int32, (32, 160), 0)
    col = lax.broadcasted_iota(jnp.int32, (32, 160), 1)
    back = row + 128 - col
    allowed = (back >= 0) & (back <= 128) & ((col >> 5) + spi >= 4)
    for r in range(16):
        at = slice(r * 32, (r + 1) * 32)
        later = slice(ROWS + r * 32, ROWS + (r + 1) * 32)
        key = jnp.concatenate([x[at] for x in (x4, x3, x2, x1, x0)], axis=0)
        value = jnp.concatenate([x[later] for x in (x4, x3, x2, x1, x0)], axis=0)
        out, log_total = attend(q3_ref[at], key, value, allowed)
        out_ref[pl.ds(r, 32, stride=16), :] = out
        log_ref[pl.ds(r, 32, stride=16), :] = jnp.broadcast_to(log_total, (32, DH))


def merge_body(spi_ref, q_ref, own_ref, send_ref, halo_ref, out3_ref, log3_ref, merged_ref, out2, log2, out1, log1):
    spi = spi_ref[0, 0]
    row = lax.broadcasted_iota(jnp.int32, (128, 256), 0)
    col = lax.broadcasted_iota(jnp.int32, (128, 256), 1)
    back = row + 128 - col
    inside = (back >= 0) & (back <= 128)
    edge = inside & ((col >= 128) | (spi >= 1))
    for r in range(4):
        at = slice(256 + r * 128, 256 + (r + 1) * 128)
        later = slice(256 + ROWS + r * 128, 256 + ROWS + (r + 1) * 128)
        key = jnp.concatenate([halo_ref[at], send_ref[at]], axis=0)
        value = jnp.concatenate([halo_ref[later], send_ref[later]], axis=0)
        out, log_total = attend(q_ref[ROWS + r * 128 : ROWS + (r + 1) * 128], key, value, edge)
        out2[pl.ds(r, 128, stride=4), :] = out
        log2[pl.ds(r, 128, stride=4), :] = jnp.broadcast_to(log_total, (128, DH))
    for b in range(4):
        if b == 0:
            key = jnp.concatenate([halo_ref[:128], own_ref[:128]], axis=0)
            value = jnp.concatenate([halo_ref[128:256], own_ref[ROWS : ROWS + 128]], axis=0)
        else:
            key = own_ref[(b - 1) * 128 : (b + 1) * 128]
            value = own_ref[ROWS + (b - 1) * 128 : ROWS + (b + 1) * 128]
        at = slice(b * 128, (b + 1) * 128)
        out, log_total = attend(q_ref[at], key, value, edge if b == 0 else inside)
        l1 = jnp.broadcast_to(log_total, (128, DH))
        out1[at] = out
        log1[at] = l1
    for b in range(4):
        at = slice(b * 128, (b + 1) * 128)
        l1, l2, l3 = log1[at], log2[at], log3_ref[at]
        top = jnp.maximum(jnp.maximum(l1, l2), l3)
        e1, e2, e3 = jnp.exp(l1 - top), jnp.exp(l2 - top), jnp.exp(l3 - top)
        merged = (e1 * out1[at] + e2 * out2[at] + e3 * out3_ref[at]) / (e1 + e2 + e3)
        merged_ref[at] = merged.astype(BF16)


def out_body(m_ref, w_ref, out_ref):
    left = jnp.concatenate([m_ref[h] for h in range(4)], axis=1)
    for z in range(8):
        heads = []
        for h in range(4):
            pieces = [
                w_ref[h, z * 256 + c * 128 + y * 16 : z * 256 + c * 128 + y * 16 + 16, :]
                for y in range(8)
                for c in range(2)
            ]
            heads.append(jnp.concatenate(pieces, axis=0))
        right = jnp.concatenate(heads, axis=1)
        out_ref[:, z * 256 : (z + 1) * 256] = lax.dot_general(
            left, right, (((1,), (1,)), ((), ())), preferred_element_type=F32
        ).astype(BF16)


def shape(rows, cols, dtype=BF16):
    return jax.ShapeDtypeStruct((rows, cols), dtype)


def on_device(tokens, w_query, w_key, w_value, w_out):
    spi = lax.axis_index(SP).astype(jnp.int32)
    core = lax.axis_index("core")
    vmem = pl.BlockSpec(memory_space=pltpu.VMEM)
    smem = pl.BlockSpec(memory_space=pltpu.SMEM)
    stage = pltpu.VMEM((ROWS, DH), F32)

    packed = jnp.concatenate(
        [w_key[:, :256], w_value[:, :256], w_query, w_out.T, w_key[:, 256:], w_value[:, 256:]], axis=1
    )
    line = spread(packed, "y").reshape(128, 1280)
    plane = lax.all_gather(line[:, :1024], ("z", "core"), axis=0, tiled=True)
    third = spread(spread(line[:, 1024:], "z"), "core")

    cos, sin = tables(spi * ROWS)
    tok = call(reorder_body, shape(ROWS, 2048), flops=2 * ROWS * 2048 * 256, moved=4 * MIB, name="reorder")(tokens)

    x0 = call(
        kv3_body, shape(2 * ROWS, DH), [stage], 2 * ROWS * 2048 * 256, 4 * MIB, "kv3"
    )(tok, third, cos, sin)
    x2 = from_behind(x0, 2)
    x4 = from_behind(x2, 2)
    x1 = from_partner(jnp.where(core == 0, x0, x2))
    x3 = from_partner(jnp.where(core == 0, x2, x4))

    own, send = call(
        kv12_body,
        (shape(2 * ROWS, DH), shape(1280, DH)),
        [stage],
        2 * ROWS * 2048 * 512,
        5 * MIB,
        "kv12",
    )(tok, plane[:, :512], cos, sin)
    halo = from_behind(send, 1)
    spi_cell = spi.reshape(1, 1)
    queries, out3, log3 = call(
        q_body,
        (shape(2 * ROWS, DH), shape(ROWS, DH, F32), shape(ROWS, DH, F32)),
        [stage, pltpu.VMEM((ROWS, DH), BF16)],
        2 * ROWS * 2048 * 384,
        6 * MIB,
        "q",
        [smem] + [vmem] * 9,
    )(spi_cell, tok, plane[:, 512:896], cos, sin, x4, x3, x2, x1, x0)
    merged = call(
        merge_body,
        shape(ROWS, DH),
        [stage] * 4,
        8 * 4 * 128 * 256 * 128,
        3 * MIB,
        "merge",
        [smem] + [vmem] * 6,
    )(spi_cell, queries, own, send, halo, out3, log3)

    all_heads = spread(plane[:, 896:], "tp")
    by_position = lax.all_to_all(merged.reshape(4, 128, DH), "tp", split_axis=0, concat_axis=0, tiled=True)
    return call(out_body, shape(128, 2048), flops=2 * 128 * 512 * 2048, moved=3 * MIB, name="project")(
        by_position, all_heads
    )


def solution(mesh):
    grid = Mesh(mesh.devices.reshape(8, 8, 2, 4), (*SP, "tp"))
    placed = (P(SP, None), P(SP, "tp"), P(SP, "tp"), P(SP, "tp"), P("tp", SP))
    return jax.shard_map(
        on_device, mesh=grid, in_specs=placed, out_specs=P((*SP, "tp"), None), check_vma=False
    )
```

time: 197 us -> 159 us (0.81)
  the two profiles are of different devices: /device:TPU:1 before, /device:TPU:64 now
where the time goes in v1:
time: 159 us
  blocking collectives  52.5 us (33%)
  waiting for transfers between devices  41.9 us (26%)
  starting transfers between devices  24.3 us (15%)
  Pallas kernels  14.5 us (9%)
  between operations  13.6 us (9%)
  local copies, waits for them, and re-layouts  9.72 us (6%)
  other arithmetic  2.04 us (1%)
    all_to_all x3, blocking collectives, spread(): return lax.all_to_all(copies, axis, split_axis=0, concat_axis=0, tiled=True)  52.5 us
    ppermute x3, waiting for transfers between devices, from_behind(): lax.ppermute(block, SP, [(i - distance, i) for i in range(distance, size)])  20.2 us
    all_to_all x1, waiting for transfers between devices, spread(): return lax.all_to_all(copies, axis, split_axis=0, concat_axis=0, tiled=True)  15.7 us
    all_to_all x1, starting transfers between devices, spread(): return lax.all_to_all(copies, axis, split_axis=0, concat_axis=0, tiled=True)  9.96 us
    pallas_call x1, Pallas kernels, on_device(): call(q_body, (shape(2 * ROWS, DH), shape(ROWS, DH, F32), shape(ROWS, DH,...  8.09 us
    all_to_all x1, waiting for transfers between devices, on_device(): lax.all_to_all(merged.reshape(4, 128, DH), 'tp', split_axis=0, concat_axi...  5.98 us
    ppermute x3, starting transfers between devices, from_behind(): lax.ppermute(block, SP, [(i - distance, i) for i in range(distance, size)])  5.75 us
    unnamed x11, local copies, waits for them, and re-layouts  5.09 us
  transfers between devices with their start and end apart: 8, of which 5 were waited for; matrix products, arithmetic and copies ran while one was open for 3% of the time, Pallas kernels for 7%

profile of v1, /device:TPU:64, one launch (start us, length us, event | category | flops | bytes accessed | tf_op | source)
XLA Modules:
  0.0 158.6 jit_solution(15322311452579061451)
XLA Ops:
  6.5 0.7 constant_dynamic-update-slice_fusion.5
  7.2 0.7 constant_dynamic-update-slice_fusion.4
  7.9 0.7 constant_dynamic-update-slice_fusion.3
  8.6 0.7 constant_dynamic-update-slice_fusion.2
  9.3 0.7 constant_dynamic-update-slice_fusion.1
  10.0 0.7 constant_dynamic-update-slice_fusion
  10.8 20.2 %all_to_all.25 = bf16[8,16,1280]{2,1,0:T(8,128)(2,1)S(1)} all-to-all(bf16[8,16,1280]{2,1,0:T(8,128)(2,1)S(1)} %broadcast_in_dim.14), channel_id=1, replica_groups=mesh['z'=8,'y'=8,'core'=2,'tp'=4] {'y'}, dimensions={0} | all-to-all | bytes 655360 | tf_op jit(solution)/shard_map/all_to_all | solution.py:23
  30.9 0.7 slice.36
  31.7 0.8 broadcast_in_dim.15
  32.5 10.0 %all-to-all-start.1 = ((bf16[8,128,256]{2,1,0:T(8,128)(2,1)}), bf16[8,128,256]{2,1,0:T(8,128)(2,1)S(1)}, u32[]{:S(2)}, u32[]{:S(2)}) async-start(bf16[8,128,256]{2,1,0:T(8,128)(2,1)} %broadcast_in_dim.15), calls=%async_computation.1 | async-start | bytes 1048576 | tf_op jit(solution)/shard_map/all_to_all | solution.py:23
  42.5 1.6 %copy-done.1 = bf16[512,2048]{1,0:T(8,128)(2,1)S(1)} copy-done((bf16[512,2048]{1,0:T(8,128)(2,1)S(1)}, bf16[512,2048]{1,0:T(8,128)(2,1)}, u32[]{:S(2)}) %copy-start.1) | copy-done | bytes 2097176
  44.1 0.7 reorder.1.tok_ref
  44.9 1.0 fusion
  46.1 15.7 %all-to-all-done.1 = bf16[8,128,256]{2,1,0:T(8,128)(2,1)S(1)} async-done(((bf16[8,128,256]{2,1,0:T(8,128)(2,1)}), bf16[8,128,256]{2,1,0:T(8,128)(2,1)S(1)}, u32[]{:S(2)}, u32[]{:S(2)}) %all-to-all-start.1) | async-done | bytes 524320 | tf_op jit(solution)/shard_map/all_to_all | solution.py:23
  61.9 4.7 %all_to_all.26.w_ref = bf16[2,8,128,256]{3,2,1,0:T(8,128)(2,1)S(1)} all-to-all(bf16[2,8,128,256]{3,2,1,0:T(8,128)(2,1)S(1)} %broadcast_in_dim.16), channel_id=1, replica_groups=mesh['z'=8,'y'=8,'core'=2,'tp'=4] {'core'}, dimensions={0} | all-to-all | bytes 2097152 | tf_op jit(solution)/shard_map/all_to_all | solution.py:23
  66.5 0.9 kv3.1.x0
  67.4 1.9 %collective-permute-start = (bf16[1024,128]{1,0:T(8,128)(2,1)S(1)}, bf16[1024,128]{1,0:T(8,128)(2,1)S(1)}, u32[]{:S(2)}, u32[]{:S(2)}) collective-permute-start(bf16[1024,128]{1,0:T(8,128)(2,1)S(1)} %kv3.1.x0), channel_id=1, source_target_pairs={{0,8},{4,12},{8,16},{12,20},{16,24},{20,28},{24,32},{28,36},{32,40... | collective-permute-start | bytes 786440 | tf_op jit(solution)/shard_map/ppermute | solution.py:28
  69.4 10.5 %collective-permute-done.x2 = bf16[1024,128]{1,0:T(8,128)(2,1)S(1)} collective-permute-done((bf16[1024,128]{1,0:T(8,128)(2,1)S(1)}, bf16[1024,128]{1,0:T(8,128)(2,1)S(1)}, u32[]{:S(2)}, u32[]{:S(2)}) %collective-permute-start) | collective-permute-done | bytes 262176 | tf_op jit(solution)/shard_map/ppermute | solution.py:28
  79.9 1.9 %collective-permute-start.1 = (bf16[1024,128]{1,0:T(8,128)(2,1)S(1)}, bf16[1024,128]{1,0:T(8,128)(2,1)S(1)}, u32[]{:S(2)}, u32[]{:S(2)}) collective-permute-start(bf16[1024,128]{1,0:T(8,128)(2,1)S(1)} %collective-permute-done.x2), channel_id=1, source_target_pairs={{0,8},{4,12},{8,16},{12,20},{16,24},{20,28},{24,32},{28,36},{32,40... | collective-permute-start | bytes 786440 | tf_op jit(solution)/shard_map/ppermute | solution.py:28
  81.8 9.5 %collective-permute-done.1.x4 = bf16[1024,128]{1,0:T(8,128)(2,1)S(1)} collective-permute-done((bf16[1024,128]{1,0:T(8,128)(2,1)S(1)}, bf16[1024,128]{1,0:T(8,128)(2,1)S(1)}, u32[]{:S(2)}, u32[]{:S(2)}) %collective-permute-start.1) | collective-permute-done | bytes 262176 | tf_op jit(solution)/shard_map/ppermute | solution.py:28
  91.3 0.8 broadcast_select_fusion
  92.2 1.9 %collective-permute-start.2 = (bf16[1024,128]{1,0:T(8,128)(2,1)}, bf16[1024,128]{1,0:T(8,128)(2,1)}, u32[]{:S(2)}, u32[]{:S(2)}) collective-permute-start(bf16[1024,128]{1,0:T(8,128)(2,1)} %get-tuple-element.16), channel_id=1, source_target_pairs={{0,4},{4,0},{1,5},{5,1},{2,6},{6,2},{3,7},{7,3},{8,12},{12,8},{9,1... | collective-permute-start | bytes 786440 | tf_op jit(solution)/shard_map/ppermute | solution.py:32
  94.1 2.4 %collective-permute-start.3 = (bf16[1024,128]{1,0:T(8,128)(2,1)}, bf16[1024,128]{1,0:T(8,128)(2,1)}, u32[]{:S(2)}, u32[]{:S(2)}) collective-permute-start(bf16[1024,128]{1,0:T(8,128)(2,1)} %get-tuple-element.15), channel_id=1, source_target_pairs={{0,4},{4,0},{1,5},{5,1},{2,6},{6,2},{3,7},{7,3},{8,12},{12,8},{9,1... | collective-permute-start | bytes 786440 | tf_op jit(solution)/shard_map/ppermute | solution.py:32
  96.5 1.7 %slice.39.w_ref = bf16[2048,512]{1,0:T(8,128)(2,1)S(1)} slice(bf16[2048,1024]{1,0:T(8,128)(2,1)} %all-gather.2.cloned.1.call-done), slice={[0:2048], [0:512]} | slice | bytes 4194304 | tf_op jit(solution)/shard_map/slice | solution.py:221
  98.3 1.4 kv12.1
  99.6 1.9 %collective-permute-start.4 = (bf16[1280,128]{1,0:T(8,128)(2,1)S(1)}, bf16[1280,128]{1,0:T(8,128)(2,1)S(1)}, u32[]{:S(2)}, u32[]{:S(2)}) collective-permute-start(bf16[1280,128]{1,0:T(8,128)(2,1)S(1)} %get-tuple-element.12.send_ref), channel_id=1, source_target_pairs={{0,4},{4,8},{8,12},{12,16},{16,20},{20,24},{24,28},{28,32},{32,36}... | collective-permute-start | bytes 983048 | tf_op jit(solution)/shard_map/ppermute | solution.py:28
  101.8 8.1 %q.1 = (bf16[1024,128]{1,0:T(8,128)(2,1)S(1)}, f32[512,128]{1,0:T(8,128)S(1)}, f32[512,128]{1,0:T(8,128)S(1)}) custom-call(s32[1,1]{1,0:T(1,128)} %bitcast.spi_ref, bf16[512,2048]{1,0:T(8,128)(2,1)} %copy-done, bf16[2048,384]{1,0:T(8,128)(2,1)S(1)} %slice.37.w_ref, f32[512,128]{1,0:T(8,128)S(1)} %get-tuple-element.20.cos_ref, ...), custom_call_target="tpu_custom_call" | custom-call | flops 805306368 | bytes 6291456 | tf_op jit(solution)/shard_map/q/pallas_call | solution.py:224
  110.1 1.8 %merge.1 = bf16[512,128]{1,0:T(8,128)(2,1)} custom-call(s32[1,1]{1,0:T(1,128)} %bitcast.spi_ref, bf16[1024,128]{1,0:T(8,128)(2,1)S(1)} %get-tuple-element.10.q_ref, bf16[1024,128]{1,0:T(8,128)(2,1)S(1)} %get-tuple-element.11.own_ref, bf16[1280,128]{1,0:T(8,128)(2,1)S(1)} %get-tuple-element.12.send_ref, ...), custom_call_target="tpu_custom_call" | custom-call | flops 134217728 | bytes 3145728 | tf_op jit(solution)/shard_map/merge/pallas_call | solution.py:233
  111.9 4.3 %all-to-all-start.3 = ((bf16[4,128,128]{2,1,0:T(8,128)(2,1)}), bf16[4,128,128]{2,1,0:T(8,128)(2,1)S(1)}, u32[]{:S(2)}, u32[]{:S(2)}) async-start(bf16[4,128,128]{2,1,0:T(8,128)(2,1)} %bitcast.3), calls=%async_computation.3 | async-start | bytes 262144 | tf_op jit(solution)/shard_map/all_to_all | solution.py:244
  116.2 6.0 %all-to-all-done.3.m_ref = bf16[4,128,128]{2,1,0:T(8,128)(2,1)S(1)} async-done(((bf16[4,128,128]{2,1,0:T(8,128)(2,1)}), bf16[4,128,128]{2,1,0:T(8,128)(2,1)S(1)}, u32[]{:S(2)}, u32[]{:S(2)}) %all-to-all-start.3) | async-done | bytes 131104 | tf_op jit(solution)/shard_map/all_to_all | solution.py:244
  122.5 27.6 %all_to_all.27.w_ref = bf16[4,2048,128]{2,1,0:T(8,128)(2,1)S(1)} all-to-all(bf16[4,2048,128]{2,1,0:T(8,128)(2,1)S(1)} %broadcast_in_dim.17), channel_id=1, replica_groups=mesh['z'=8,'y'=8,'core'=2,'tp'=4] {'tp'}, dimensions={0} | all-to-all | bytes 4194304 | tf_op jit(solution)/shard_map/all_to_all | solution.py:23
  150.1 1.6 %project.1 = bf16[128,2048]{1,0:T(8,128)(2,1)} custom-call(bf16[4,128,128]{2,1,0:T(8,128)(2,1)S(1)} %all-to-all-done.3.m_ref, bf16[4,2048,128]{2,1,0:T(8,128)(2,1)S(1)} %all_to_all.27.w_ref), custom_call_target="tpu_custom_call" | custom-call | flops 268435456 | bytes 3145728 | tf_op jit(solution)/shard_map/project/pallas_call | solution.py:245
  (21 shorter events, 1.1 us)
Async XLA Ops:
  6.5 90.0 %all-gather.2.cloned.1.call-start = ((), (), s32[]{:S(2)}) async-start(), calls=%async_computation.5 | async-start | bytes 4456448 | tf_op jit(solution)/shard_map/all_gather | solution.py:200
  32.5 29.2 %all-to-all-start.1 = ((bf16[8,128,256]{2,1,0:T(8,128)(2,1)}), bf16[8,128,256]{2,1,0:T(8,128)(2,1)S(1)}, u32[]{:S(2)}, u32[]{:S(2)}) async-start(bf16[8,128,256]{2,1,0:T(8,128)(2,1)} %broadcast_in_dim.15), calls=%async_computation.1 | async-start | bytes 1048576 | tf_op jit(solution)/shard_map/all_to_all | solution.py:23
  42.5 1.6 %copy-start.1 = (bf16[512,2048]{1,0:T(8,128)(2,1)S(1)}, bf16[512,2048]{1,0:T(8,128)(2,1)}, u32[]{:S(2)}) copy-start(bf16[512,2048]{1,0:T(8,128)(2,1)} %tok_ref.1) | copy-start | bytes 6291460
  44.8 53.4 %copy-start = (bf16[512,2048]{1,0:T(8,128)(2,1)}, bf16[512,2048]{1,0:T(8,128)(2,1)S(1)}, u32[]{:S(2)}) copy-start(bf16[512,2048]{1,0:T(8,128)(2,1)S(1)} %reorder.1.tok_ref) | copy-start | bytes 6291460
  67.4 12.4 %collective-permute-start = (bf16[1024,128]{1,0:T(8,128)(2,1)S(1)}, bf16[1024,128]{1,0:T(8,128)(2,1)S(1)}, u32[]{:S(2)}, u32[]{:S(2)}) collective-permute-start(bf16[1024,128]{1,0:T(8,128)(2,1)S(1)} %kv3.1.x0), channel_id=1, source_target_pairs={{0,8},{4,12},{8,16},{12,20},{16,24},{20,28},{24,32},{28,36},{32,40... | collective-permute-start | bytes 786440 | tf_op jit(solution)/shard_map/ppermute | solution.py:28
  79.9 11.4 %collective-permute-start.1 = (bf16[1024,128]{1,0:T(8,128)(2,1)S(1)}, bf16[1024,128]{1,0:T(8,128)(2,1)S(1)}, u32[]{:S(2)}, u32[]{:S(2)}) collective-permute-start(bf16[1024,128]{1,0:T(8,128)(2,1)S(1)} %collective-permute-done.x2), channel_id=1, source_target_pairs={{0,8},{4,12},{8,16},{12,20},{16,24},{20,28},{24,32},{28,36},{32,40... | collective-permute-start | bytes 786440 | tf_op jit(solution)/shard_map/ppermute | solution.py:28
  92.2 9.7 %collective-permute-start.2 = (bf16[1024,128]{1,0:T(8,128)(2,1)}, bf16[1024,128]{1,0:T(8,128)(2,1)}, u32[]{:S(2)}, u32[]{:S(2)}) collective-permute-start(bf16[1024,128]{1,0:T(8,128)(2,1)} %get-tuple-element.16), channel_id=1, source_target_pairs={{0,4},{4,0},{1,5},{5,1},{2,6},{6,2},{3,7},{7,3},{8,12},{12,8},{9,1... | collective-permute-start | bytes 786440 | tf_op jit(solution)/shard_map/ppermute | solution.py:32
  94.1 7.8 %collective-permute-start.3 = (bf16[1024,128]{1,0:T(8,128)(2,1)}, bf16[1024,128]{1,0:T(8,128)(2,1)}, u32[]{:S(2)}, u32[]{:S(2)}) collective-permute-start(bf16[1024,128]{1,0:T(8,128)(2,1)} %get-tuple-element.15), channel_id=1, source_target_pairs={{0,4},{4,0},{1,5},{5,1},{2,6},{6,2},{3,7},{7,3},{8,12},{12,8},{9,1... | collective-permute-start | bytes 786440 | tf_op jit(solution)/shard_map/ppermute | solution.py:32
  98.3 3.3 %copy-start.2 = (bf16[2048,1024]{1,0:T(8,128)(2,1)S(1)}, bf16[2048,1024]{1,0:T(8,128)(2,1)}, u32[]{:S(2)}) copy-start(bf16[2048,1024]{1,0:T(8,128)(2,1)} %all-gather.2.cloned.1.call-done) | copy-start | bytes 12582916
  99.6 10.5 %collective-permute-start.4 = (bf16[1280,128]{1,0:T(8,128)(2,1)S(1)}, bf16[1280,128]{1,0:T(8,128)(2,1)S(1)}, u32[]{:S(2)}, u32[]{:S(2)}) collective-permute-start(bf16[1280,128]{1,0:T(8,128)(2,1)S(1)} %get-tuple-element.12.send_ref), channel_id=1, source_target_pairs={{0,4},{4,8},{8,12},{12,16},{16,20},{20,24},{24,28},{28,32},{32,36}... | collective-permute-start | bytes 983048 | tf_op jit(solution)/shard_map/ppermute | solution.py:28
  109.9 12.3 %slice-start = ((bf16[2048,1024]{1,0:T(8,128)(2,1)}), bf16[2048,128]{1,0:T(8,128)(2,1)S(1)}, s32[]{:S(2)}) async-start(bf16[2048,1024]{1,0:T(8,128)(2,1)} %all-gather.2.cloned.1.call-done), calls=%async_computation.6 | async-start | bytes 1048576 | tf_op jit(solution)/shard_map/slice | solution.py:243
  111.9 10.3 %all-to-all-start.3 = ((bf16[4,128,128]{2,1,0:T(8,128)(2,1)}), bf16[4,128,128]{2,1,0:T(8,128)(2,1)S(1)}, u32[]{:S(2)}, u32[]{:S(2)}) async-start(bf16[4,128,128]{2,1,0:T(8,128)(2,1)} %bitcast.3), calls=%async_computation.3 | async-start | bytes 262144 | tf_op jit(solution)/shard_map/all_to_all | solution.py:244
Sparse Core Ops, SparseCore 0:
  31.8 52.7 all-gather.1

commit v2 on v1

--- a/solution.py
+++ b/solution.py
@@ -1,5 +1,3 @@
-import functools
-
 import jax
 import jax.numpy as jnp
 from jax import lax
@@ -38,7 +36,7 @@
         body,
         out_shape=outs,
         scratch_shapes=list(scratch),
-        compiler_params=pltpu.CompilerParams(vmem_limit_bytes=48 * MIB),
+        compiler_params=pltpu.CompilerParams(vmem_limit_bytes=24 * MIB),
         cost_estimate=pl.CostEstimate(flops=flops, bytes_accessed=moved, transcendentals=0),
         name=name,
         **extra,
@@ -67,6 +65,25 @@
         out_ref[:, z * 256 : (z + 1) * 256] = jnp.dot(part, moves, preferred_element_type=F32).astype(BF16)
 
 
+def pack_body(q_ref, k_ref, v_ref, o_ref, out_ref):
+    for y in range(8):
+        out_ref[y, :, 0:256] = k_ref[:, :256]
+        out_ref[y, :, 256:512] = v_ref[:, :256]
+        for h in range(4):
+            out_ref[y, :, 512 + h * DH : 512 + (h + 1) * DH] = o_ref[h]
+        out_ref[y, :, 1024:1408] = q_ref[...]
+        out_ref[y, :, 1408:1536] = k_ref[:, 256:]
+        out_ref[y, :, 1536:1664] = v_ref[:, 256:]
+
+
+def unpack_body(line_ref, most_ref, third_ref):
+    for y in range(8):
+        at = slice(y * 16, (y + 1) * 16)
+        most_ref[at] = line_ref[y, :, :1408]
+        for z in range(8):
+            third_ref[z, at] = line_ref[y, :, 1408:]
+
+
 def by_residue(value, stage_ref, out_ref, base, stride):
     stage_ref[...] = value
     count = ROWS // stride
@@ -85,12 +102,18 @@
     by_residue(acc[:, DH:], stage_ref, out_ref, ROWS, 16)
 
 
-def kv12_body(tok_ref, w_ref, cos_ref, sin_ref, own_ref, send_ref, stage_ref):
+def kv12_body(tok_ref, plane_ref, cos_ref, sin_ref, own_ref, send_ref, stage_ref, w_ref, key_sem, value_sem):
+    key_copy = pltpu.make_async_copy(plane_ref.at[:, : 2 * DH], w_ref.at[:, : 2 * DH], key_sem)
+    value_copy = pltpu.make_async_copy(plane_ref.at[:, 2 * DH : 4 * DH], w_ref.at[:, 2 * DH :], value_sem)
+    key_copy.start()
+    value_copy.start()
+    key_copy.wait()
     keys = jnp.dot(tok_ref[...], w_ref[:, : 2 * DH], preferred_element_type=F32)
     near = turned(keys[:, :DH], cos_ref, sin_ref).astype(BF16)
     own_ref[:ROWS] = near
     send_ref[:128] = near[ROWS - 128 :]
     by_residue(turned(keys[:, DH:], cos_ref, sin_ref), stage_ref, send_ref, 256, 4)
+    value_copy.wait()
     values = jnp.dot(tok_ref[...], w_ref[:, 2 * DH :], preferred_element_type=F32)
     near = values[:, :DH].astype(BF16)
     own_ref[ROWS:] = near
@@ -98,35 +121,58 @@
     by_residue(values[:, DH:], stage_ref, send_ref, 256 + ROWS, 4)
 
 
-def attend(query, key, value, allowed):
-    scores = lax.dot_general(query, key, (((1,), (1,)), ((), ())), preferred_element_type=F32) * SCALE
-    scores = jnp.where(allowed, scores, -jnp.inf)
+def product(query, key):
+    return lax.dot_general(query, key, (((1,), (1,)), ((), ())), preferred_element_type=F32)
+
+
+def shares(scores, allowed):
+    scores = jnp.where(allowed, scores * SCALE, -jnp.inf)
     top = jnp.max(scores, axis=-1, keepdims=True)
     weight = jnp.exp(scores - top)
     total = jnp.sum(weight, axis=-1, keepdims=True)
-    probs = (weight * (1.0 / total)).astype(BF16)
-    return jnp.dot(probs, value, preferred_element_type=F32), top + jnp.log(total)
-
-
-def q_body(spi_ref, tok_ref, w_ref, cos_ref, sin_ref, x4, x3, x2, x1, x0, q_ref, out_ref, log_ref, stage_ref, q3_ref):
+    return (weight * (1.0 / total)).astype(BF16), top + jnp.log(total)
+
+
+def attend(query, key, value, allowed):
+    probs, log_total = shares(product(query, key), allowed)
+    return jnp.dot(probs, value, preferred_element_type=F32), log_total
+
+
+def q_body(
+    spi_ref, tok_ref, plane_ref, cos_ref, sin_ref, x4, x3, x2, x1, x0, q_ref, out_ref, log_ref,
+    stage_ref, q3_ref, w_ref, first_sem, third_sem,
+):
+    third_copy = pltpu.make_async_copy(plane_ref.at[:, 1280:1408], w_ref.at[:, 256:], third_sem)
+    first_copy = pltpu.make_async_copy(plane_ref.at[:, 1024:1280], w_ref.at[:, :256], first_sem)
+    third_copy.start()
+    first_copy.start()
     spi = spi_ref[0, 0]
-    first = jnp.dot(tok_ref[...], w_ref[:, : 2 * DH], preferred_element_type=F32)
+    third_copy.wait()
+    third = jnp.dot(tok_ref[...], w_ref[:, 256:], preferred_element_type=F32)
+    by_residue(turned(third, cos_ref, sin_ref), stage_ref, q3_ref, 0, 16)
+    first_copy.wait()
+    first = jnp.dot(tok_ref[...], w_ref[:, :256], preferred_element_type=F32)
     q_ref[:ROWS] = turned(first[:, :DH], cos_ref, sin_ref).astype(BF16)
     by_residue(turned(first[:, DH:], cos_ref, sin_ref), stage_ref, q_ref, ROWS, 4)
-    third = jnp.dot(tok_ref[...], w_ref[:, 2 * DH : 3 * DH], preferred_element_type=F32)
-    by_residue(turned(third, cos_ref, sin_ref), stage_ref, q3_ref, 0, 16)
-    row = lax.broadcasted_iota(jnp.int32, (32, 160), 0)
-    col = lax.broadcasted_iota(jnp.int32, (32, 160), 1)
+    row = lax.broadcasted_iota(jnp.int32, (ROWS, 160), 0) & 31
+    col = lax.broadcasted_iota(jnp.int32, (ROWS, 160), 1)
     back = row + 128 - col
     allowed = (back >= 0) & (back <= 128) & ((col >> 5) + spi >= 4)
+    scores = []
     for r in range(16):
         at = slice(r * 32, (r + 1) * 32)
+        key = jnp.concatenate([x[at] for x in (x4, x3, x2, x1, x0)], axis=0)
+        scores.append(product(q3_ref[at], key))
+    probs, log_total = shares(jnp.concatenate(scores, axis=0), allowed)
+    wide = jnp.broadcast_to(log_total, (ROWS, DH))
+    outs = []
+    for r in range(16):
         later = slice(ROWS + r * 32, ROWS + (r + 1) * 32)
-        key = jnp.concatenate([x[at] for x in (x4, x3, x2, x1, x0)], axis=0)
         value = jnp.concatenate([x[later] for x in (x4, x3, x2, x1, x0)], axis=0)
-        out, log_total = attend(q3_ref[at], key, value, allowed)
-        out_ref[pl.ds(r, 32, stride=16), :] = out
-        log_ref[pl.ds(r, 32, stride=16), :] = jnp.broadcast_to(log_total, (32, DH))
+        outs.append(jnp.dot(probs[r * 32 : (r + 1) * 32], value, preferred_element_type=F32))
+    for r in range(16):
+        out_ref[pl.ds(r, 32, stride=16), :] = outs[r]
+        log_ref[pl.ds(r, 32, stride=16), :] = wide[r * 32 : (r + 1) * 32]
 
 
 def merge_body(spi_ref, q_ref, own_ref, send_ref, halo_ref, out3_ref, log3_ref, merged_ref, out2, log2, out1, log1):
@@ -165,21 +211,19 @@
         merged_ref[at] = merged.astype(BF16)
 
 
-def out_body(m_ref, w_ref, out_ref):
+def out_body(m_ref, plane_ref, out_ref, w_ref, sem):
+    copy = pltpu.make_async_copy(plane_ref.at[:, 512:1024], w_ref, sem)
+    copy.start()
     left = jnp.concatenate([m_ref[h] for h in range(4)], axis=1)
+    copy.wait()
     for z in range(8):
-        heads = []
-        for h in range(4):
-            pieces = [
-                w_ref[h, z * 256 + c * 128 + y * 16 : z * 256 + c * 128 + y * 16 + 16, :]
-                for y in range(8)
-                for c in range(2)
-            ]
-            heads.append(jnp.concatenate(pieces, axis=0))
-        right = jnp.concatenate(heads, axis=1)
-        out_ref[:, z * 256 : (z + 1) * 256] = lax.dot_general(
-            left, right, (((1,), (1,)), ((), ())), preferred_element_type=F32
-        ).astype(BF16)
+        pieces = []
+        for y in range(8):
+            for c in range(2):
+                start = z * 256 + c * 128 + y * 16
+                pieces.append(w_ref[start : start + 16, :])
+        right = jnp.concatenate(pieces, axis=0)
+        out_ref[:, z * 256 : (z + 1) * 256] = product(left, right).astype(BF16)
 
 
 def shape(rows, cols, dtype=BF16):
@@ -191,14 +235,20 @@
     core = lax.axis_index("core")
     vmem = pl.BlockSpec(memory_space=pltpu.VMEM)
     smem = pl.BlockSpec(memory_space=pltpu.SMEM)
+    anywhere = pl.BlockSpec(memory_space=pltpu.HBM)
+    dma = pltpu.SemaphoreType.DMA
     stage = pltpu.VMEM((ROWS, DH), F32)
 
-    packed = jnp.concatenate(
-        [w_key[:, :256], w_value[:, :256], w_query, w_out.T, w_key[:, 256:], w_value[:, 256:]], axis=1
+    heads = spread(w_out.T, "tp")
+    packed = call(pack_body, jax.ShapeDtypeStruct((8, 16, 1664), BF16), moved=MIB, name="pack")(
+        w_query, w_key, w_value, heads
     )
-    line = spread(packed, "y").reshape(128, 1280)
-    plane = lax.all_gather(line[:, :1024], ("z", "core"), axis=0, tiled=True)
-    third = spread(spread(line[:, 1024:], "z"), "core")
+    line = lax.all_to_all(packed, "y", split_axis=0, concat_axis=0, tiled=True)
+    most, third = call(
+        unpack_body, (shape(128, 1408), jax.ShapeDtypeStruct((8, 128, 256), BF16)), moved=MIB, name="unpack"
+    )(line)
+    plane = lax.all_gather(most, ("z", "core"), axis=0, tiled=True)
+    third = spread(lax.all_to_all(third, "z", split_axis=0, concat_axis=0, tiled=True), "core")
 
     cos, sin = tables(spi * ROWS)
     tok = call(reorder_body, shape(ROWS, 2048), flops=2 * ROWS * 2048 * 256, moved=4 * MIB, name="reorder")(tokens)
@@ -214,22 +264,23 @@
     own, send = call(
         kv12_body,
         (shape(2 * ROWS, DH), shape(1280, DH)),
-        [stage],
+        [stage, pltpu.VMEM((2048, 512), BF16), dma, dma],
         2 * ROWS * 2048 * 512,
         5 * MIB,
         "kv12",
-    )(tok, plane[:, :512], cos, sin)
+        [vmem, anywhere, vmem, vmem],
+    )(tok, plane, cos, sin)
     halo = from_behind(send, 1)
     spi_cell = spi.reshape(1, 1)
     queries, out3, log3 = call(
         q_body,
         (shape(2 * ROWS, DH), shape(ROWS, DH, F32), shape(ROWS, DH, F32)),
-        [stage, pltpu.VMEM((ROWS, DH), BF16)],
+        [stage, pltpu.VMEM((ROWS, DH), BF16), pltpu.VMEM((2048, 384), BF16), dma, dma],
         2 * ROWS * 2048 * 384,
         6 * MIB,
         "q",
-        [smem] + [vmem] * 9,
-    )(spi_cell, tok, plane[:, 512:896], cos, sin, x4, x3, x2, x1, x0)
+        [smem, vmem, anywhere] + [vmem] * 7,
+    )(spi_cell, tok, plane, cos, sin, x4, x3, x2, x1, x0)
     merged = call(
         merge_body,
         shape(ROWS, DH),
@@ -240,11 +291,16 @@
         [smem] + [vmem] * 6,
     )(spi_cell, queries, own, send, halo, out3, log3)
 
-    all_heads = spread(plane[:, 896:], "tp")
     by_position = lax.all_to_all(merged.reshape(4, 128, DH), "tp", split_axis=0, concat_axis=0, tiled=True)
-    return call(out_body, shape(128, 2048), flops=2 * 128 * 512 * 2048, moved=3 * MIB, name="project")(
-        by_position, all_heads
-    )
+    return call(
+        out_body,
+        shape(128, 2048),
+        [pltpu.VMEM((2048, 512), BF16), dma],
+        2 * 128 * 512 * 2048,
+        3 * MIB,
+        "project",
+        [vmem, anywhere],
+    )(by_position, plane)
 
 
 def solution(mesh):

time: 159 us -> 138 us (0.87)
  blocking collectives: 52.5 us -> 43.4 us
  starting transfers between devices: 24.3 us -> 20 us
  waiting for transfers between devices: 41.9 us -> 38.5 us
  local copies, waits for them, and re-layouts: 9.72 us -> 7.19 us
  Pallas kernels: 14.5 us -> 12.8 us
    all_to_all x3 -> x2, blocking collectives: 52.5 us -> 14.1 us  [spread(): return lax.all_to_all(copies, axis, split_axis=0, concat_axis=0, tiled=True)]
    all_to_all x0 -> x2, blocking collectives: none -> 29.2 us  [the longest x1 20.9 us: on_device(): line = lax.all_to_all(packed, 'y', split_axis=0, concat_axis=0, tiled=True)]
    all_to_all x2 -> x1, waiting for transfers between devices: 21.7 us -> 14.2 us  [on_device(): lax.all_to_all(third, 'z', split_axis=0, concat_axis=0, tiled=True)]
    all_to_all x2 -> x1, starting transfers between devices: 14.3 us -> 9.98 us  [on_device(): lax.all_to_all(third, 'z', split_axis=0, concat_axis=0, tiled=True)]
    ppermute x3, waiting for transfers between devices: 20.2 us -> 24.2 us  [from_behind(): lax.ppermute(block, SP, [(i - distance, i) for i in range(distance, size)])]
    pallas_call x1, Pallas kernels: 8.09 us -> 4.42 us  [on_device(): call(q_body, (shape(2 * ROWS, DH), shape(ROWS, DH, F32), shape(ROWS, DH,...]
    slice x6 -> x0, local copies, waits for them, and re-layouts: 2.71 us -> none  [the longest x1 1.73 us: on_device(): plane[:, :512]]
    pallas_call x2 -> x4, Pallas kernels: 2.97 us -> 5.57 us  [the longest x1 2.76 us: on_device(): call(kv12_body, (shape(2 * ROWS, DH), shape(1280, DH)), [stage, pltpu.VME...]
  transfers between devices with their start and end apart: 8 -> 7, of which waited for: 5 -> 4; matrix products, arithmetic and copies ran while one was open for 3% -> 2% of each run, Pallas kernels for 7% -> 6%
where the time goes in v2:
time: 138 us; the launch traced here: 137 us
  blocking collectives  43.4 us (31%)
  waiting for transfers between devices  38.5 us (28%)
  starting transfers between devices  20 us (14%)
  between operations  13.6 us (10%)
  Pallas kernels  12.8 us (9%)
  local copies, waits for them, and re-layouts  7.19 us (5%)
  other arithmetic  2.05 us (1%)
    ppermute x3, waiting for transfers between devices, from_behind(): lax.ppermute(block, SP, [(i - distance, i) for i in range(distance, size)])  24.2 us
    all_to_all x1, blocking collectives, on_device(): line = lax.all_to_all(packed, 'y', split_axis=0, concat_axis=0, tiled=True)  20.9 us
    all_to_all x1, waiting for transfers between devices, on_device(): lax.all_to_all(third, 'z', split_axis=0, concat_axis=0, tiled=True)  14.2 us
    all_to_all x2, blocking collectives, spread(): return lax.all_to_all(copies, axis, split_axis=0, concat_axis=0, tiled=True)  14.1 us
    all_to_all x1, starting transfers between devices, on_device(): lax.all_to_all(third, 'z', split_axis=0, concat_axis=0, tiled=True)  9.98 us
    all_to_all x1, blocking collectives, on_device(): lax.all_to_all(merged.reshape(4, 128, DH), 'tp', split_axis=0, concat_axi...  8.36 us
    unnamed x12, local copies, waits for them, and re-layouts  6.4 us
    ppermute x3, starting transfers between devices, from_behind(): lax.ppermute(block, SP, [(i - distance, i) for i in range(distance, size)])  5.75 us
  transfers between devices with their start and end apart: 7, of which 4 were waited for; matrix products, arithmetic and copies ran while one was open for 2% of the time, Pallas kernels for 6%

profile of v2, /device:TPU:64, one launch (start us, length us, event | category | flops | bytes accessed | tf_op | source)
XLA Modules:
  0.0 137.5 jit_solution(14900016014582989181)
XLA Ops:
  6.5 0.7 broadcast_in_dim.8
  7.2 9.4 %all_to_all.25.o_ref = bf16[4,16,128]{2,1,0:T(8,128)(2,1)S(1)} all-to-all(bf16[4,16,128]{2,1,0:T(8,128)(2,1)S(1)} %broadcast_in_dim.8), channel_id=1, replica_groups=mesh['z'=8,'y'=8,'core'=2,'tp'=4] {'tp'}, dimensions={0} | all-to-all | bytes 32768 | tf_op jit(solution)/shard_map/all_to_all | solution.py:21
  16.7 0.7 copy-done.3
  17.4 0.7 copy-done.4
  18.1 0.7 copy-done.5
  18.8 20.9 %all_to_all.26.line_ref = bf16[8,16,1664]{2,1,0:T(8,128)(2,1)S(1)} all-to-all(bf16[8,16,1664]{2,1,0:T(8,128)(2,1)S(1)} %pack.1), channel_id=1, replica_groups=mesh['z'=8,'y'=8,'core'=2,'tp'=4] {'y'}, dimensions={0} | all-to-all | bytes 851968 | tf_op jit(solution)/shard_map/all_to_all | solution.py:246
  39.7 1.0 unpack.1
  40.7 10.0 %all-to-all-start.2 = ((bf16[8,128,256]{2,1,0:T(8,128)(2,1)}), bf16[8,128,256]{2,1,0:T(8,128)(2,1)S(1)}, u32[]{:S(2)}, u32[]{:S(2)}) async-start(bf16[8,128,256]{2,1,0:T(8,128)(2,1)} %get-tuple-element.13), calls=%async_computation.2 | async-start | bytes 1048576 | tf_op jit(solution)/shard_map/all_to_all | solution.py:251
  50.7 1.6 %copy-done.2 = bf16[512,2048]{1,0:T(8,128)(2,1)S(1)} copy-done((bf16[512,2048]{1,0:T(8,128)(2,1)S(1)}, bf16[512,2048]{1,0:T(8,128)(2,1)}, u32[]{:S(2)}) %copy-start.2) | copy-done | bytes 2097176
  52.3 0.7 reorder.1.tok_ref
  53.1 1.0 fusion
  54.1 0.2 pad_maximum_fusion
  54.3 14.2 %all-to-all-done.2 = bf16[8,128,256]{2,1,0:T(8,128)(2,1)S(1)} async-done(((bf16[8,128,256]{2,1,0:T(8,128)(2,1)}), bf16[8,128,256]{2,1,0:T(8,128)(2,1)S(1)}, u32[]{:S(2)}, u32[]{:S(2)}) %all-to-all-start.2) | async-done | bytes 524320 | tf_op jit(solution)/shard_map/all_to_all | solution.py:251
  68.5 0.1 broadcast_in_dim.9
  68.6 4.7 %all_to_all.27.w_ref = bf16[2,8,128,256]{3,2,1,0:T(8,128)(2,1)S(1)} all-to-all(bf16[2,8,128,256]{3,2,1,0:T(8,128)(2,1)S(1)} %broadcast_in_dim.9), channel_id=1, replica_groups=mesh['z'=8,'y'=8,'core'=2,'tp'=4] {'core'}, dimensions={0} | all-to-all | bytes 2097152 | tf_op jit(solution)/shard_map/all_to_all | solution.py:21
  73.3 0.9 kv3.1.x0
  74.2 1.9 %collective-permute-start = (bf16[1024,128]{1,0:T(8,128)(2,1)S(1)}, bf16[1024,128]{1,0:T(8,128)(2,1)S(1)}, u32[]{:S(2)}, u32[]{:S(2)}) collective-permute-start(bf16[1024,128]{1,0:T(8,128)(2,1)S(1)} %kv3.1.x0), channel_id=1, source_target_pairs={{0,8},{4,12},{8,16},{12,20},{16,24},{20,28},{24,32},{28,36},{32,40... | collective-permute-start | bytes 786440 | tf_op jit(solution)/shard_map/ppermute | solution.py:26
  76.1 10.5 %collective-permute-done.x2 = bf16[1024,128]{1,0:T(8,128)(2,1)S(1)} collective-permute-done((bf16[1024,128]{1,0:T(8,128)(2,1)S(1)}, bf16[1024,128]{1,0:T(8,128)(2,1)S(1)}, u32[]{:S(2)}, u32[]{:S(2)}) %collective-permute-start) | collective-permute-done | bytes 262176 | tf_op jit(solution)/shard_map/ppermute | solution.py:26
  86.7 1.9 %collective-permute-start.1 = (bf16[1024,128]{1,0:T(8,128)(2,1)S(1)}, bf16[1024,128]{1,0:T(8,128)(2,1)S(1)}, u32[]{:S(2)}, u32[]{:S(2)}) collective-permute-start(bf16[1024,128]{1,0:T(8,128)(2,1)S(1)} %collective-permute-done.x2), channel_id=1, source_target_pairs={{0,8},{4,12},{8,16},{12,20},{16,24},{20,28},{24,32},{28,36},{32,40... | collective-permute-start | bytes 786440 | tf_op jit(solution)/shard_map/ppermute | solution.py:26
  88.6 9.6 %collective-permute-done.1.x4 = bf16[1024,128]{1,0:T(8,128)(2,1)S(1)} collective-permute-done((bf16[1024,128]{1,0:T(8,128)(2,1)S(1)}, bf16[1024,128]{1,0:T(8,128)(2,1)S(1)}, u32[]{:S(2)}, u32[]{:S(2)}) %collective-permute-start.1) | collective-permute-done | bytes 262176 | tf_op jit(solution)/shard_map/ppermute | solution.py:26
  98.2 0.8 broadcast_select_fusion
  99.0 1.9 %collective-permute-start.3 = (bf16[1024,128]{1,0:T(8,128)(2,1)}, bf16[1024,128]{1,0:T(8,128)(2,1)}, u32[]{:S(2)}, u32[]{:S(2)}) collective-permute-start(bf16[1024,128]{1,0:T(8,128)(2,1)} %get-tuple-element.19), channel_id=1, source_target_pairs={{0,4},{4,0},{1,5},{5,1},{2,6},{6,2},{3,7},{7,3},{8,12},{12,8},{9,1... | collective-permute-start | bytes 786440 | tf_op jit(solution)/shard_map/ppermute | solution.py:30
  100.9 2.4 %collective-permute-start.2 = (bf16[1024,128]{1,0:T(8,128)(2,1)}, bf16[1024,128]{1,0:T(8,128)(2,1)}, u32[]{:S(2)}, u32[]{:S(2)}) collective-permute-start(bf16[1024,128]{1,0:T(8,128)(2,1)} %get-tuple-element.20), channel_id=1, source_target_pairs={{0,4},{4,0},{1,5},{5,1},{2,6},{6,2},{3,7},{7,3},{8,12},{12,8},{9,1... | collective-permute-start | bytes 786440 | tf_op jit(solution)/shard_map/ppermute | solution.py:30
  103.4 0.0 all-gather.2.cloned.1.call-done.plane_ref
  103.4 2.6 %copy-done = bf16[2048,1408]{1,0:T(8,128)(2,1)S(1)} copy-done((bf16[2048,1408]{1,0:T(8,128)(2,1)S(1)}, bf16[2048,1408]{1,0:T(8,128)(2,1)}, u32[]{:S(2)}) %copy-start) | copy-done | bytes 5767192
  106.0 2.8 %kv12.1 = (bf16[1024,128]{1,0:T(8,128)(2,1)S(1)}, bf16[1280,128]{1,0:T(8,128)(2,1)S(1)}) custom-call(bf16[512,2048]{1,0:T(8,128)(2,1)S(1)} %reorder.1.tok_ref, bf16[2048,1408]{1,0:T(8,128)(2,1)S(1)} %copy-done, f32[512,128]{1,0:T(8,128)S(1)} %get-tuple-element.24.cos_ref, f32[512,128]{1,0:T(8,128)S(1)} %get-tuple-element.25.sin_ref), custom_call_target="tpu_custom_call" | custom-call | flops 1073741824 | bytes 5242880 | tf_op jit(solution)/shard_map/kv12/pallas_call | solution.py:264
  108.8 1.9 %collective-permute-start.4 = (bf16[1280,128]{1,0:T(8,128)(2,1)S(1)}, bf16[1280,128]{1,0:T(8,128)(2,1)S(1)}, u32[]{:S(2)}, u32[]{:S(2)}) collective-permute-start(bf16[1280,128]{1,0:T(8,128)(2,1)S(1)} %get-tuple-element.16.send_ref), channel_id=1, source_target_pairs={{0,4},{4,8},{8,12},{12,16},{16,20},{20,24},{24,28},{28,32},{32,36}... | collective-permute-start | bytes 983048 | tf_op jit(solution)/shard_map/ppermute | solution.py:26
  110.8 4.4 %q.1 = (bf16[1024,128]{1,0:T(8,128)(2,1)S(1)}, f32[512,128]{1,0:T(8,128)S(1)}, f32[512,128]{1,0:T(8,128)S(1)}) custom-call(s32[1,1]{1,0:T(1,128)} %bitcast.spi_ref, bf16[512,2048]{1,0:T(8,128)(2,1)S(1)} %reorder.1.tok_ref, bf16[2048,1408]{1,0:T(8,128)(2,1)S(1)} %copy-done.1, f32[512,128]{1,0:T(8,128)S(1)} %get-tuple-element.24.cos_ref, ...), custom_call_target="tpu_custom_call" | custom-call | flops 805306368 | bytes 6291456 | tf_op jit(solution)/shard_map/q/pallas_call | solution.py:275
  115.2 4.1 %collective-permute-done.4.halo_ref = bf16[1280,128]{1,0:T(8,128)(2,1)S(1)} collective-permute-done((bf16[1280,128]{1,0:T(8,128)(2,1)S(1)}, bf16[1280,128]{1,0:T(8,128)(2,1)S(1)}, u32[]{:S(2)}, u32[]{:S(2)}) %collective-permute-start.4) | collective-permute-done | bytes 327712 | tf_op jit(solution)/shard_map/ppermute | solution.py:26
  119.3 1.2 merge.1
  120.5 8.4 %all_to_all.28.m_ref = bf16[4,128,128]{2,1,0:T(8,128)(2,1)S(1)} all-to-all(bf16[4,128,128]{2,1,0:T(8,128)(2,1)S(1)} %bitcast.3), channel_id=1, replica_groups=mesh['z'=8,'y'=8,'core'=2,'tp'=4] {'tp'}, dimensions={0} | all-to-all | bytes 262144 | tf_op jit(solution)/shard_map/all_to_all | solution.py:294
  128.8 1.8 %project.1 = bf16[128,2048]{1,0:T(8,128)(2,1)} custom-call(bf16[4,128,128]{2,1,0:T(8,128)(2,1)S(1)} %all_to_all.28.m_ref, bf16[2048,1408]{1,0:T(8,128)(2,1)S(1)} %copy-done.1), custom_call_target="tpu_custom_call" | custom-call | flops 268435456 | bytes 3145728 | tf_op jit(solution)/shard_map/project/pallas_call | solution.py:295
  (14 shorter events, 0.1 us)
Async XLA Ops:
  6.5 96.8 %all-gather.2.cloned.1.call-start = ((), (), s32[]{:S(2)}) async-start(), calls=%async_computation.5 | async-start | bytes 6127616 | tf_op jit(solution)/shard_map/all_gather | solution.py:250
  16.7 0.7 copy-start.3
  17.4 0.7 copy-start.4
  18.1 0.7 copy-start.5
  40.7 27.8 %all-to-all-start.2 = ((bf16[8,128,256]{2,1,0:T(8,128)(2,1)}), bf16[8,128,256]{2,1,0:T(8,128)(2,1)S(1)}, u32[]{:S(2)}, u32[]{:S(2)}) async-start(bf16[8,128,256]{2,1,0:T(8,128)(2,1)} %get-tuple-element.13), calls=%async_computation.2 | async-start | bytes 1048576 | tf_op jit(solution)/shard_map/all_to_all | solution.py:251
  50.7 1.7 %copy-start.2 = (bf16[512,2048]{1,0:T(8,128)(2,1)S(1)}, bf16[512,2048]{1,0:T(8,128)(2,1)}, u32[]{:S(2)}) copy-start(bf16[512,2048]{1,0:T(8,128)(2,1)} %tok_ref.1) | copy-start | bytes 6291460
  74.2 12.4 %collective-permute-start = (bf16[1024,128]{1,0:T(8,128)(2,1)S(1)}, bf16[1024,128]{1,0:T(8,128)(2,1)S(1)}, u32[]{:S(2)}, u32[]{:S(2)}) collective-permute-start(bf16[1024,128]{1,0:T(8,128)(2,1)S(1)} %kv3.1.x0), channel_id=1, source_target_pairs={{0,8},{4,12},{8,16},{12,20},{16,24},{20,28},{24,32},{28,36},{32,40... | collective-permute-start | bytes 786440 | tf_op jit(solution)/shard_map/ppermute | solution.py:26
  86.7 11.5 %collective-permute-start.1 = (bf16[1024,128]{1,0:T(8,128)(2,1)S(1)}, bf16[1024,128]{1,0:T(8,128)(2,1)S(1)}, u32[]{:S(2)}, u32[]{:S(2)}) collective-permute-start(bf16[1024,128]{1,0:T(8,128)(2,1)S(1)} %collective-permute-done.x2), channel_id=1, source_target_pairs={{0,8},{4,12},{8,16},{12,20},{16,24},{20,28},{24,32},{28,36},{32,40... | collective-permute-start | bytes 786440 | tf_op jit(solution)/shard_map/ppermute | solution.py:26
  99.0 11.7 %collective-permute-start.3 = (bf16[1024,128]{1,0:T(8,128)(2,1)}, bf16[1024,128]{1,0:T(8,128)(2,1)}, u32[]{:S(2)}, u32[]{:S(2)}) collective-permute-start(bf16[1024,128]{1,0:T(8,128)(2,1)} %get-tuple-element.19), channel_id=1, source_target_pairs={{0,4},{4,0},{1,5},{5,1},{2,6},{6,2},{3,7},{7,3},{8,12},{12,8},{9,1... | collective-permute-start | bytes 786440 | tf_op jit(solution)/shard_map/ppermute | solution.py:30
  100.9 9.8 %collective-permute-start.2 = (bf16[1024,128]{1,0:T(8,128)(2,1)}, bf16[1024,128]{1,0:T(8,128)(2,1)}, u32[]{:S(2)}, u32[]{:S(2)}) collective-permute-start(bf16[1024,128]{1,0:T(8,128)(2,1)} %get-tuple-element.20), channel_id=1, source_target_pairs={{0,4},{4,0},{1,5},{5,1},{2,6},{6,2},{3,7},{7,3},{8,12},{12,8},{9,1... | collective-permute-start | bytes 786440 | tf_op jit(solution)/shard_map/ppermute | solution.py:30
  103.4 2.6 %copy-start = (bf16[2048,1408]{1,0:T(8,128)(2,1)S(1)}, bf16[2048,1408]{1,0:T(8,128)(2,1)}, u32[]{:S(2)}) copy-start(bf16[2048,1408]{1,0:T(8,128)(2,1)} %all-gather.2.cloned.1.call-done.plane_ref) | copy-start | bytes 17301508
  106.0 4.7 %copy-start.1 = (bf16[2048,1408]{1,0:T(8,128)(2,1)S(1)}, bf16[2048,1408]{1,0:T(8,128)(2,1)}, u32[]{:S(2)}) copy-start(bf16[2048,1408]{1,0:T(8,128)(2,1)} %all-gather.2.cloned.1.call-done.plane_ref) | copy-start | bytes 17301508
  108.8 10.5 %collective-permute-start.4 = (bf16[1280,128]{1,0:T(8,128)(2,1)S(1)}, bf16[1280,128]{1,0:T(8,128)(2,1)S(1)}, u32[]{:S(2)}, u32[]{:S(2)}) collective-permute-start(bf16[1280,128]{1,0:T(8,128)(2,1)S(1)} %get-tuple-element.16.send_ref), channel_id=1, source_target_pairs={{0,4},{4,8},{8,12},{12,16},{16,20},{20,24},{24,28},{28,32},{32,36}... | collective-permute-start | bytes 983048 | tf_op jit(solution)/shard_map/ppermute | solution.py:26
Sparse Core Ops, SparseCore 0:
  40.8 60.2 all-gather.1
